TPU v7x, 32 devices: a whole 2x2x4 slice. The times are simulated.
32 devices in a mesh: sp: 8 (over z, y), tp: 4 (over x, core).
Axes of the slice: x: 2, y: 2, z: 4, core: 2. Of those that a mesh axis runs over, the one named last changes fastest.
Arguments:
- tokens: bfloat16 [4096, 2048], P('sp', 'tp'), may hold values from -400 to 400
- norm_gain: float32 [2048], replicated, may hold values from 0.1 to 1.9
- query_weight: bfloat16 [2048, 1024], P(None, 'tp'), may hold values from -0.37306796 to 0.37306796
- key_weight: bfloat16 [2048, 1024], P(None, 'tp'), may hold values from -0.2625825 to 0.2625825
- value_weight: bfloat16 [2048, 1024], P(None, 'tp'), may hold values from -0.125 to 0.125
- outer_gate_weight: bfloat16 [2048, 1024], P(None, 'tp'), may hold values from -0.125 to 0.125
- inner_gate_weight: bfloat16 [2048, 1024], P(None, 'tp'), may hold values from -0.125 to 0.125
- conv_input_weight: bfloat16 [2048, 1024], P(None, 'tp'), may hold values from -0.125 to 0.125
- conv_taps: float32 [3, 1024], P(None, 'tp'), may hold values from -3.5 to 3.5
- lambdas: float32 [8], P('tp'), may hold values from 0.3 to 0.8
- head_gain: float32 [128], replicated, may hold values from 0.1 to 1.9
- attn_out_weight: bfloat16 [1024, 2048], P(None, 'tp'), may hold values from -0.125 to 0.125
- conv_out_weight: bfloat16 [1024, 2048], P(None, 'tp'), may hold values from -0.125 to 0.125
Outputs:
- mixed_out: bfloat16 [4096, 2048], P('sp', 'tp')
- log_totals: float32 [8, 2, 4096], P('tp', None, 'sp')
All inputs are finite; a program needn't handle non-finite values.
Results may differ from a plain program's by a relative error of at most 0.014.
The roundings to bfloat16 on the way count: a program that leaves them out, or rounds other values in their place, can miss the bound.
Values may be sent and summed in bfloat16 or wider, within the bound.
A program may use at most 128 MiB of HBM per device.

v0:
```python
import math

import jax
import jax.numpy as jnp
from jax import lax
from jax.sharding import PartitionSpec as P

NORM_EPS = 1e-06
HEAD_EPS = 1e-05
ROPE_BASE = 500000.0
MASKED = -1e30
HEAD_SCALE = 0.8


def shifted(block, axis, distance):
    devices = range(lax.axis_size(axis))
    route = [(i - distance, i) for i in devices if i - distance in devices]
    return lax.ppermute(block, axis, route)


def rotate(field_in, positions):
    half_dim = field_in.shape[-1] // 2
    frequency = ROPE_BASE ** (-jnp.arange(half_dim, dtype=jnp.float32) * 2.0 / field_in.shape[-1])
    angles = positions[:, None] * frequency[None, :]
    cosine = jnp.cos(angles)[:, None, None, :]
    sine_part = jnp.sin(angles)[:, None, None, :]
    first_half = field_in[..., :half_dim]
    second_half = field_in[..., half_dim:]
    return jnp.concatenate(
        [
            first_half * cosine - second_half * sine_part,
            second_half * cosine + first_half * sine_part,
        ],
        axis=-1,
    )


def add_products(block_in, norm_gain, weights):
    floats = block_in.astype(jnp.float32)
    scaled = (floats * norm_gain[None, :]).astype(jnp.bfloat16)
    products = tuple(
        (jnp.dot(scaled, weight, preferred_element_type=jnp.float32) for weight in weights)
    )
    return (jnp.sum(floats * floats, axis=1, keepdims=True),) + products


def over_shards(step_fn, running, arrays, anchor, local_rows):
    shard_count = arrays[0].shape[0] // local_rows
    group_size = math.gcd(shard_count, max(1, 2048 // local_rows))
    block_rows = group_size * local_rows
    steps_count = shard_count // group_size
    stacked = tuple(
        (member.reshape((steps_count, block_rows) + member.shape[1:]) for member in arrays)
    )

    def scan_step(carried, scan_items):
        members, step_index = scan_items
        return (step_fn(carried, members, anchor + step_index * block_rows), None)

    result, unused = lax.scan(
        scan_step, running, (stacked, jnp.arange(steps_count, dtype=jnp.int32))
    )
    return result


def per_device(
    tokens,
    norm_gain,
    query_weight,
    key_weight,
    value_weight,
    outer_gate_weight,
    inner_gate_weight,
    conv_input_weight,
    conv_taps,
    lambdas,
    head_gain,
    attn_out_weight,
    conv_out_weight,
):
    local_rows = tokens.shape[0]
    local_heads = lambdas.shape[0]
    head_dim = query_weight.shape[1] // (2 * local_heads)
    value_dim = 2 * head_dim
    taps_count = conv_taps.shape[0]
    width_all = norm_gain.shape[0]
    columns_dev = query_weight.shape[1]
    attn_weights = (query_weight, key_weight, value_weight)
    conv_weights = (outer_gate_weight, inner_gate_weight, conv_input_weight)
    squares, query_raw, key_raw, value_raw, outer_raw, inner_raw, signal_raw = add_products(
        lax.all_gather(tokens, "tp", axis=1, tiled=True), norm_gain, attn_weights + conv_weights
    )
    inverse_rms = lax.rsqrt(squares / width_all + NORM_EPS)
    query_pos = lax.axis_index("sp") * local_rows + jnp.arange(local_rows, dtype=jnp.int32)
    positions = query_pos.astype(jnp.float32)
    queries = rotate(
        (inverse_rms * query_raw).reshape(local_rows, local_heads, 2, head_dim), positions
    ).astype(jnp.bfloat16)
    key_rows = rotate(
        (inverse_rms * key_raw).reshape(local_rows, local_heads, 2, head_dim), positions
    ).astype(jnp.bfloat16)
    values = (
        (inverse_rms * value_raw).astype(jnp.bfloat16).reshape(local_rows, local_heads, value_dim)
    )
    outer_gate = (inverse_rms * outer_raw).astype(jnp.bfloat16)
    inner_gate = (inverse_rms * inner_raw).astype(jnp.bfloat16)
    signal = (inverse_rms * signal_raw).astype(jnp.bfloat16)
    conv_in = (inner_gate.astype(jnp.float32) * signal.astype(jnp.float32)).astype(jnp.bfloat16)
    rim_rows = shifted(conv_in[local_rows - (taps_count - 1) :], "sp", 1)
    padded = jnp.concatenate([rim_rows, conv_in], axis=0)
    summed = jnp.zeros((local_rows, columns_dev), jnp.float32)
    for tap_index in range(taps_count):
        summed = summed + conv_taps[tap_index][None, :] * padded[
            tap_index : tap_index + local_rows
        ].astype(jnp.float32)
    conv_out = (outer_gate.astype(jnp.float32) * summed).astype(jnp.bfloat16)
    scale_factor = head_dim ** (-0.5)

    def block_scores(key_block, key_anchor):
        scores = (
            jnp.einsum("qhcd,khcd->hcqk", queries, key_block, preferred_element_type=jnp.float32)
            * scale_factor
        )
        visible = (
            query_pos[:, None]
            >= (key_anchor + jnp.arange(key_block.shape[0], dtype=jnp.int32))[None, :]
        )
        return (jnp.where(visible, scores, MASKED), visible)

    def stats_step(running, members, key_anchor):
        max_before, sum_before = running
        scores, visible = block_scores(members[0], key_anchor)
        max_after = jnp.maximum(max_before, jnp.max(scores, axis=-1))
        exponent = jnp.where(visible, jnp.exp(scores - max_after[..., None]), 0.0)
        return (
            max_after,
            sum_before * jnp.exp(max_before - max_after) + jnp.sum(exponent, axis=-1),
        )

    stats_init = (
        jnp.full((local_heads, 2, local_rows), MASKED, jnp.float32),
        jnp.zeros((local_heads, 2, local_rows), jnp.float32),
    )
    value_init = jnp.zeros((local_rows, local_heads, value_dim), jnp.float32)

    def value_step_with(row_max, row_sum):

        def value_step(running, members, key_anchor):
            scores, visible = block_scores(members[0], key_anchor)
            normalized = jnp.where(
                visible, jnp.exp(scores - row_max[..., None]) / row_sum[..., None], 0.0
            )
            weights = (normalized[:, 0] - lambdas[:, None, None] * normalized[:, 1]).astype(
                jnp.bfloat16
            )
            return running + jnp.einsum(
                "hqk,khv->qhv", weights, members[1], preferred_element_type=jnp.float32
            )

        return value_step

    all_keys, all_values = (
        lax.all_gather(key_rows, "sp", axis=0, tiled=True),
        lax.all_gather(values, "sp", axis=0, tiled=True),
    )
    row_max, row_sum = over_shards(stats_step, stats_init, (all_keys,), 0, local_rows)
    head_mix = over_shards(
        value_step_with(row_max, row_sum), value_init, (all_keys, all_values), 0, local_rows
    )
    log_totals = row_max + jnp.log(row_sum)
    normed = (
        head_mix
        * lax.rsqrt(jnp.mean(head_mix * head_mix, axis=-1, keepdims=True) + HEAD_EPS)
        * head_gain[None, None, :]
        * HEAD_SCALE
    )
    attn_out = normed.astype(jnp.bfloat16).reshape(local_rows, local_heads * value_dim)
    running = jnp.zeros((local_rows, attn_out_weight.shape[1]), jnp.float32)
    running = jnp.dot(
        lax.all_gather(attn_out, "tp", axis=1, tiled=True),
        attn_out_weight,
        preferred_element_type=jnp.float32,
    )
    mixed_out = running + jnp.dot(
        lax.all_gather(conv_out, "tp", axis=1, tiled=True),
        conv_out_weight,
        preferred_element_type=jnp.float32,
    )
    return (mixed_out.astype(jnp.bfloat16), log_totals)


def solution(mesh):
    in_specs = (
        P("sp", "tp"),
        P(),
        P(None, "tp"),
        P(None, "tp"),
        P(None, "tp"),
        P(None, "tp"),
        P(None, "tp"),
        P(None, "tp"),
        P(None, "tp"),
        P("tp"),
        P(),
        P(None, "tp"),
        P(None, "tp"),
    )
    out_specs = (P("sp", "tp"), P("tp", None, "sp"))
    return jax.shard_map(
        per_device, mesh=mesh, in_specs=in_specs, out_specs=out_specs, check_vma=False
    )
```

profile of v0, /device:TPU:25, one launch (start us, length us, event | category | flops | bytes accessed | tf_op | source)
XLA Modules:
  0.0 209.9 jit_solution(9740739602610465239)
XLA Ops:
  7.2 0.0 copy-start
  7.2 0.0 copy-start.16
  7.2 0.0 all-gather.6.cloned.1.call-start
  7.2 0.7 all-gather.6.cloned.1.call-update
  7.9 0.0 all-gather.10.cloned.1.call-start
  8.0 0.3 multiply_cosine_fusion
  8.3 25.2 %all-gather.6.cloned.1.call-done = bf16[512,2048]{1,0:T(8,128)(2,1)} async-done(((bf16[512,512]{1,0:T(8,128)(2,1)}), bf16[512,2048]{1,0:T(8,128)(2,1)}) %all-gather.6.cloned.1.call-update) | async-done | bytes 2097168 | tf_op jit(solution)/shard_map/all_gather | solution.py:91
  33.5 2.2 %fusion.32 = f32[512]{0:T(512)S(1)} fusion(bf16[512,2048]{1,0:T(8,128)(2,1)} %all-gather.6.cloned.1.call-done), kind=kLoop, calls=%fused_computation.40 | loop fusion | flops 3145216 | bytes 2099200 | tf_op jit(solution)/shard_map/reduce_sum | solution.py:44
  35.8 2.6 %convolution_multiply_fusion.4 = f32[512,256]{0,1:T(8,128)S(1)} fusion(bf16[2048,256]{1,0:T(8,128)(2,1)} %param.20, bf16[512,2048]{1,0:T(8,128)(2,1)} %all-gather.6.cloned.1.call-done, f32[2048]{0:T(1024)} %param.18, f32[512]{0:T(512)S(1)} %add_rsqrt_fusion.1), kind=kOutput, calls=%fused_computation.49 | convolution fusion | flops 540147712 | bytes 3680256 | tf_op jit(solution)/shard_map/dot_general | solution.py:42
  38.4 0.8 convolution_multiply_fusion.3
  39.2 0.2 subtract_convert_fusion
  39.4 0.7 pad_maximum_fusion.1
  40.1 0.0 all-gather.10.cloned.1.call-update
  40.2 0.0 all-gather.8.cloned.1.call-start
  40.3 2.7 %fusion.35 = bf16[512,256]{0,1:T(8,128)(2,1)} fusion(bf16[2048,256]{1,0:T(8,128)(2,1)} %param.21, bf16[512,2048]{1,0:T(8,128)(2,1)S(1)} %copy-done.1, f32[2048]{0:T(1024)} %param.18, f32[512]{0:T(512)S(1)} %add_rsqrt_fusion.1), kind=kOutput, calls=%fused_computation.51 | convolution fusion | flops 540278784 | bytes 3418112 | tf_op jit(solution)/shard_map/dot_general | solution.py:42
  42.9 1.8 copy.21
  44.7 0.0 all-gather.8.cloned.1.call-update
  44.8 0.0 all-gather.12.cloned.1.call-start
  44.8 0.7 pad_maximum_fusion.2
  45.5 42.9 %all-gather.10.cloned.1.call-done = bf16[4096,2,2,64]{0,3,2,1:T(8,128)(2,1)} async-done(((bf16[512,2,2,64]{0,3,2,1:T(8,128)(2,1)}), bf16[4096,2,2,64]{0,3,2,1:T(8,128)(2,1)}) %all-gather.10.cloned.1.call-update) | async-done | bytes 2097168 | tf_op jit(solution)/shard_map/all_gather | solution.py:163
  88.5 1.7 copy.34
  90.2 0.0 copy-start.18
  90.2 18.7 %while.24 = (s32[]{:T(128)}, f32[2,2,512]{2,1,0:T(2,128)S(1)}, f32[2,2,512]{2,1,0:T(2,128)S(1)}, s32[2]{0:T(128)S(1)}, bf16[2,2048,2,2,64]{1,4,3,2,0:T(8,128)(2,...) while((s32[]{:T(128)}, f32[2,2,512]{2,1,0:T(2,128)S(1)}, ...), condition=%wide.region_4.5_spmd.clone, body=%wide.region_1.4_spmd.clone.sunk | while | flops 571486720 | bytes 38138008 | solution.py:60
  90.3 0.6 dynamic_slice.43
  91.5 0.8 broadcast_compare_fusion.4
  92.3 3.0 %fusion.78 = (f32[2,2,512]{2,1,0:T(2,128)S(1)}, f32[2,2,2048,512]{3,2,1,0:T(8,128)S(1)}) fusion(pred[512,2048]{0,1:T(8,128)(4,1)S(1)} %broadcast_compare_fusion.4, bf16[512,2,2,64]{0,3,2,1:T(8,128)(2,1)S(1)} %get-tuple-element.355, bf16[2,2048,2,2,64]{1,4,3,2,0:T(8,128)(2,1)S(1)} %get-tuple-element.354, s32[]{:T(128)S(6)} %copy.38), kind=kOutput, calls=%fused_computation.4.clone.1 | convolution fusion | flops 549451776 | bytes 19144708 | tf_op jit(solution)/shard_map/while/body/eval_jaxpr/qhcd,khcd->hcqk/dot_general | solution.py:121
  95.3 4.2 %select_reduce_fusion.2 = f32[2,2,512]{2,1,0:T(2,128)S(1)} fusion(f32[2,2,2048,512]{3,2,1,0:T(8,128)S(1)} %get-tuple-element.319, f32[2,2,512]{2,1,0:T(2,128)S(1)} %fusion.79, pred[512,2048]{0,1:T(8,128)(4,1)S(1)} %broadcast_compare_fusion.4), kind=kLoop, calls=%fused_computation.3.clone.1 | loop fusion | flops 20969472 | bytes 17842176 | tf_op jit(solution)/shard_map/while/body/eval_jaxpr/reduce_sum | solution.py:137
  99.6 0.6 dynamic_slice.43
  100.9 0.8 broadcast_compare_fusion.4
  101.7 3.0 %fusion.78 = (f32[2,2,512]{2,1,0:T(2,128)S(1)}, f32[2,2,2048,512]{3,2,1,0:T(8,128)S(1)}) fusion(pred[512,2048]{0,1:T(8,128)(4,1)S(1)} %broadcast_compare_fusion.4, bf16[512,2,2,64]{0,3,2,1:T(8,128)(2,1)S(1)} %get-tuple-element.355, bf16[2,2048,2,2,64]{1,4,3,2,0:T(8,128)(2,1)S(1)} %get-tuple-element.354, s32[]{:T(128)S(6)} %copy.38), kind=kOutput, calls=%fused_computation.4.clone.1 | convolution fusion | flops 549451776 | bytes 19144708 | tf_op jit(solution)/shard_map/while/body/eval_jaxpr/qhcd,khcd->hcqk/dot_general | solution.py:121
  104.7 4.2 %select_reduce_fusion.2 = f32[2,2,512]{2,1,0:T(2,128)S(1)} fusion(f32[2,2,2048,512]{3,2,1,0:T(8,128)S(1)} %get-tuple-element.319, f32[2,2,512]{2,1,0:T(2,128)S(1)} %fusion.79, pred[512,2048]{0,1:T(8,128)(4,1)S(1)} %broadcast_compare_fusion.4), kind=kLoop, calls=%fused_computation.3.clone.1 | loop fusion | flops 20969472 | bytes 17842176 | tf_op jit(solution)/shard_map/while/body/eval_jaxpr/reduce_sum | solution.py:137
  108.9 28.8 %all-gather.8.cloned.1.call-done = bf16[4096,2,128]{2,0,1:T(8,128)(2,1)} async-done(((bf16[512,2,128]{2,0,1:T(8,128)(2,1)}), bf16[4096,2,128]{2,0,1:T(8,128)(2,1)}) %all-gather.8.cloned.1.call-update) | async-done | bytes 2097168 | tf_op jit(solution)/shard_map/all_gather | solution.py:164
  137.8 0.0 copy-start.9
  137.8 23.3 %while.25 = (s32[]{:T(128)}, f32[512,2,128]{0,2,1:T(8,128)}, bf16[2,2048,2,128]{3,1,0,2:T(8,128)(2,1)}, s32[2]{0:T(128)S(1)}, bf16[2,2048,2,2,64]{1,4,3,2,0:T(8,...) while((s32[]{:T(128)}, f32[512,2,128]{0,2,1:T(8,128)}, ...), condition=%wide.region_6.7_spmd.clone, body=%wide.region_5.6_spmd.clone.sunk | while | flops 1102318080 | bytes 51680008 | solution.py:60
  137.8 0.6 dynamic_slice.46
  139.1 0.8 broadcast_compare_fusion.5
  139.9 7.4 %fusion.85 = f32[2,2,512,2048]{2,3,1,0:T(8,128)S(1)} fusion(f32[2,2,512]{2,1,0:T(2,128)S(1)} %get-tuple-element.393, f32[2,2,512]{2,1,0:T(2,128)S(1)} %get-tuple-element.392, pred[512,2048]{0,1:T(8,128)(4,1)S(1)} %broadcast_compare_fusion.5, bf16[512,2,2,64]{0,3,2,1:T(8,128)(2,1)S(1)} %get-tuple-element.391, ...), kind=kOutput, calls=%fused_computation.20.clone.1 | convolution fusion | flops 557842432 | bytes 19152900 | tf_op jit(solution)/shard_map/while/body/eval_jaxpr/qhcd,khcd->hcqk/dot_general | solution.py:121
  147.3 1.3 fusion.86
  148.7 0.0 copy-start.5
  148.7 0.8 copy-done.5
  149.5 0.6 dynamic_slice.46
  150.7 0.8 broadcast_compare_fusion.5
  151.5 7.4 %fusion.85 = f32[2,2,512,2048]{2,3,1,0:T(8,128)S(1)} fusion(f32[2,2,512]{2,1,0:T(2,128)S(1)} %get-tuple-element.393, f32[2,2,512]{2,1,0:T(2,128)S(1)} %get-tuple-element.392, pred[512,2048]{0,1:T(8,128)(4,1)S(1)} %broadcast_compare_fusion.5, bf16[512,2,2,64]{0,3,2,1:T(8,128)(2,1)S(1)} %get-tuple-element.391, ...), kind=kOutput, calls=%fused_computation.20.clone.1 | convolution fusion | flops 557842432 | bytes 19152900 | tf_op jit(solution)/shard_map/while/body/eval_jaxpr/qhcd,khcd->hcqk/dot_general | solution.py:121
  159.0 1.3 fusion.86
  160.3 0.0 copy-start.5
  160.3 0.8 copy-done.5
  161.1 1.1 multiply_reduce_fusion
  162.2 1.9 multiply_convert_fusion
  164.1 0.0 all-gather.12.cloned.1.call-update
  164.1 0.0 copy-start.7
  164.1 0.2 all-gather.14.cloned.1.call-start
  164.4 0.0 copy-start.13
  164.4 2.1 %fusion.42 = f32[512,256]{0,1:T(8,128)S(1)} fusion(bf16[2048,256]{1,0:T(8,128)(2,1)} %param.23, bf16[512,2048]{1,0:T(8,128)(2,1)S(1)} %copy-done.2, f32[2048]{0:T(1024)S(1)} %copy-done.17, f32[512]{0:T(512)S(1)} %copy-done.9), kind=kOutput, calls=%fused_computation.58 | convolution fusion | flops 540409856 | bytes 3680256 | tf_op jit(solution)/shard_map/dot_general | solution.py:42
  166.5 0.8 fusion.41
  167.3 0.1 slice.54
  167.4 2.2 %collective-permute-start = (bf16[2,256]{0,1:T(8,128)(2,1)S(1)}, bf16[2,256]{0,1:T(8,128)(2,1)S(1)}, u32[]{:S(2)}, u32[]{:S(2)}) collective-permute-start(bf16[2,256]{0,1:T(8,128)(2,1)S(1)} %slice.54), channel_id=1, source_target_pairs={{0,4},{4,8},{8,12},{12,16},{16,20},{20,24},{24,28},{1,5},{5,9},{9,... | collective-permute-start | bytes 3080 | tf_op jit(solution)/shard_map/ppermute | solution.py:18
  169.6 3.7 %collective-permute-done = bf16[2,256]{0,1:T(8,128)(2,1)S(1)} collective-permute-done((bf16[2,256]{0,1:T(8,128)(2,1)S(1)}, bf16[2,256]{0,1:T(8,128)(2,1)S(1)}, u32[]{:S(2)}, u32[]{:S(2)}) %collective-permute-start) | collective-permute-done | bytes 1056 | tf_op jit(solution)/shard_map/ppermute | solution.py:18
  173.3 1.6 fusion.45
  174.9 0.0 all-gather.14.cloned.1.call-update
  175.0 0.6 log_add_fusion
  175.6 6.3 %all-gather.12.cloned.1.call-done = bf16[512,1024]{0,1:T(8,128)(2,1)} async-done(((bf16[512,256]{0,1:T(8,128)(2,1)}), bf16[512,1024]{0,1:T(8,128)(2,1)}) %all-gather.12.cloned.1.call-update) | async-done | bytes 1048592 | tf_op jit(solution)/shard_map/all_gather | solution.py:180
  181.9 2.0 fusion.54
  183.8 16.8 %all-gather.14.cloned.1.call-done = bf16[512,1024]{0,1:T(8,128)(2,1)} async-done(((bf16[512,256]{0,1:T(8,128)(2,1)}), bf16[512,1024]{0,1:T(8,128)(2,1)}) %all-gather.14.cloned.1.call-update) | async-done | bytes 1048592 | tf_op jit(solution)/shard_map/all_gather | solution.py:185
  200.6 2.8 %fusion.34 = bf16[512,512]{1,0:T(8,128)(2,1)} fusion(f32[512,512]{1,0:T(8,128)S(1)} %fusion.54, bf16[512,1024]{0,1:T(8,128)(2,1)} %all-gather.14.cloned.1.call-done, bf16[1024,512]{1,0:T(8,128)(2,1)S(1)} %copy-done.15), kind=kOutput, calls=%fused_computation.44 | convolution fusion | flops 537395200 | bytes 3670016 | tf_op jit(solution)/shard_map/dot_general | solution.py:184
  (58 shorter events, 0.3 us)
Async XLA Ops:
  7.2 174.7 %copy-start = (bf16[1024,512]{1,0:T(8,128)(2,1)S(1)}, bf16[1024,512]{1,0:T(8,128)(2,1)}, u32[]{:S(2)}) copy-start(bf16[1024,512]{1,0:T(8,128)(2,1)} %param.28) | copy-start | bytes 3145732
  7.2 31.2 %copy-start.16 = (f32[2048]{0:T(1024)S(1)}, f32[2048]{0:T(1024)}, u32[]{:S(2)}) copy-start(f32[2048]{0:T(1024)} %param.18) | copy-start | bytes 24580
  7.2 26.3 %all-gather.6.cloned.1.call-start = ((), (), s32[]{:S(2)}) async-start(), calls=%async_computation | async-start | bytes 2621440 | tf_op jit(solution)/shard_map/all_gather | solution.py:91
  7.9 80.6 %all-gather.10.cloned.1.call-start = ((), (), s32[]{:S(2)}) async-start(), calls=%async_computation.2 | async-start | bytes 2359296 | tf_op jit(solution)/shard_map/all_gather | solution.py:163
  33.5 4.9 %copy-start.1 = (bf16[512,2048]{1,0:T(8,128)(2,1)S(1)}, bf16[512,2048]{1,0:T(8,128)(2,1)}, u32[]{:S(2)}) copy-start(bf16[512,2048]{1,0:T(8,128)(2,1)} %all-gather.6.cloned.1.call-done) | copy-start | bytes 6291460
  33.5 4.9 %copy-start.12 = (bf16[2048,256]{1,0:T(8,128)(2,1)S(1)}, bf16[2048,256]{1,0:T(8,128)(2,1)}, u32[]{:S(2)}) copy-start(bf16[2048,256]{1,0:T(8,128)(2,1)} %param.19) | copy-start | bytes 3145732
  35.8 4.5 %copy-start.8 = (f32[512]{0:T(512)}, f32[512]{0:T(512)S(1)}, u32[]{:S(2)}) copy-start(f32[512]{0:T(512)S(1)} %add_rsqrt_fusion.1) | copy-start | bytes 6148
  40.2 97.6 %all-gather.8.cloned.1.call-start = ((), (), s32[]{:S(2)}) async-start(), calls=%async_computation.1 | async-start | bytes 2359296 | tf_op jit(solution)/shard_map/all_gather | solution.py:164
  44.8 137.1 %all-gather.12.cloned.1.call-start = ((), (), s32[]{:S(2)}) async-start(), calls=%async_computation.3 | async-start | bytes 1310720 | tf_op jit(solution)/shard_map/all_gather | solution.py:180
  45.5 44.7 %copy-start.6 = (bf16[512,2,2,64]{0,3,2,1:T(8,128)(2,1)S(1)}, bf16[512,2,2,64]{0,3,2,1:T(8,128)(2,1)}, u32[]{:S(2)}) copy-start(bf16[512,2,2,64]{0,3,2,1:T(8,128)(2,1)} %pad_maximum_fusion.2) | copy-start | bytes 786436
  90.2 47.5 %copy-start.18 = (f32[2]{0:T(128)S(1)}, f32[2]{0:T(128)}, u32[]{:S(2)}) copy-start(f32[2]{0:T(128)} %param.26) | copy-start | bytes 28
  108.9 28.8 %copy-start.3 = (bf16[2,2048,2,2,64]{1,4,3,2,0:T(8,128)(2,1)}, bf16[2,2048,2,2,64]{1,4,3,2,0:T(8,128)(2,1)S(1)}, u32[]{:S(2)}) copy-start(bf16[2,2048,2,2,64]{1,4,3,2,0:T(8,128)(2,1)S(1)} %get-tuple-element.405) | copy-start | bytes 6291460
  137.8 24.4 %copy-start.10 = (f32[128]{0:T(128)S(1)}, f32[128]{0:T(128)}, u32[]{:S(2)}) copy-start(f32[128]{0:T(128)} %param.27) | copy-start | bytes 1540
  137.8 26.6 %copy-start.2 = (bf16[512,2048]{1,0:T(8,128)(2,1)S(1)}, bf16[512,2048]{1,0:T(8,128)(2,1)}, u32[]{:S(2)}) copy-start(bf16[512,2048]{1,0:T(8,128)(2,1)} %all-gather.6.cloned.1.call-done) | copy-start | bytes 6291460
  137.8 26.6 %copy-start.9 = (f32[512]{0:T(512)S(1)}, f32[512]{0:T(512)}, u32[]{:S(2)}) copy-start(f32[512]{0:T(512)} %copy-done.8) | copy-start | bytes 6148
  137.8 26.6 %copy-start.17 = (f32[2048]{0:T(1024)S(1)}, f32[2048]{0:T(1024)}, u32[]{:S(2)}) copy-start(f32[2048]{0:T(1024)} %param.18) | copy-start | bytes 24580
  139.9 7.5 %copy-start.4 = (f32[512,2,128]{0,2,1:T(8,128)S(1)}, f32[512,2,128]{0,2,1:T(8,128)}, u32[]{:S(2)}) copy-start(f32[512,2,128]{0,2,1:T(8,128)} %get-tuple-element.374) | copy-start | bytes 1572868 | tf_op jit(solution)/shard_map/while
  139.9 7.5 %copy-start.11 = (bf16[2,2048,2,128]{3,1,0,2:T(8,128)(2,1)S(1)}, bf16[2,2048,2,128]{3,1,0,2:T(8,128)(2,1)}, u32[]{:S(2)}) copy-start(bf16[2,2048,2,128]{3,1,0,2:T(8,128)(2,1)} %get-tuple-element.388) | copy-start | bytes 6291460 | tf_op jit(solution)/shard_map/while
  148.7 0.8 copy-start.5
  151.5 7.4 %copy-start.4 = (f32[512,2,128]{0,2,1:T(8,128)S(1)}, f32[512,2,128]{0,2,1:T(8,128)}, u32[]{:S(2)}) copy-start(f32[512,2,128]{0,2,1:T(8,128)} %get-tuple-element.374) | copy-start | bytes 1572868 | tf_op jit(solution)/shard_map/while
  151.5 7.4 %copy-start.11 = (bf16[2,2048,2,128]{3,1,0,2:T(8,128)(2,1)S(1)}, bf16[2,2048,2,128]{3,1,0,2:T(8,128)(2,1)}, u32[]{:S(2)}) copy-start(bf16[2,2048,2,128]{3,1,0,2:T(8,128)(2,1)} %get-tuple-element.388) | copy-start | bytes 6291460 | tf_op jit(solution)/shard_map/while
  160.3 0.8 copy-start.5
  164.1 5.5 %copy-start.7 = (f32[3,256]{1,0:T(4,128)S(1)}, f32[3,256]{1,0:T(4,128)}, u32[]{:S(2)}) copy-start(f32[3,256]{1,0:T(4,128)} %param.25) | copy-start | bytes 9220
  164.1 36.5 %all-gather.14.cloned.1.call-start = ((), (), s32[]{:S(2)}) async-start(), calls=%async_computation.4 | async-start | bytes 1310720 | tf_op jit(solution)/shard_map/all_gather | solution.py:185
  164.4 2.2 %copy-start.13 = (bf16[2048,256]{1,0:T(8,128)(2,1)S(1)}, bf16[2048,256]{1,0:T(8,128)(2,1)}, u32[]{:S(2)}) copy-start(bf16[2048,256]{1,0:T(8,128)(2,1)} %param.24) | copy-start | bytes 3145732
  164.4 9.0 %copy-start.14 = (bf16[2048,256]{1,0:T(8,128)(2,1)S(1)}, bf16[2048,256]{1,0:T(8,128)(2,1)}, u32[]{:S(2)}) copy-start(bf16[2048,256]{1,0:T(8,128)(2,1)} %param.22) | copy-start | bytes 3145732
  167.4 5.9 %collective-permute-start = (bf16[2,256]{0,1:T(8,128)(2,1)S(1)}, bf16[2,256]{0,1:T(8,128)(2,1)S(1)}, u32[]{:S(2)}, u32[]{:S(2)}) collective-permute-start(bf16[2,256]{0,1:T(8,128)(2,1)S(1)} %slice.54), channel_id=1, source_target_pairs={{0,4},{4,8},{8,12},{12,16},{16,20},{20,24},{24,28},{1,5},{5,9},{9,... | collective-permute-start | bytes 3080 | tf_op jit(solution)/shard_map/ppermute | solution.py:18
  174.9 25.7 %copy-start.15 = (bf16[1024,512]{1,0:T(8,128)(2,1)S(1)}, bf16[1024,512]{1,0:T(8,128)(2,1)}, u32[]{:S(2)}) copy-start(bf16[1024,512]{1,0:T(8,128)(2,1)} %param.29) | copy-start | bytes 3145732
Sparse Core Ops, SparseCore 0:
  9.6 23.9 all-gather.5
  40.3 48.1 all-gather.9
  90.7 47.0 all-gather.7
  164.2 17.6 all-gather.11
  183.9 16.6 all-gather.13
where the time goes:
time: 212 us; the launch traced here: 210 us
  waiting for transfers between devices  124 us (58%)
  matrix products  38.8 us (18%)
  other arithmetic  19.3 us (9%)
  between operations  14.1 us (7%)
  local copies, waits for them, and re-layouts  7.83 us (4%)
  loops' own time  2.83 us (1%)
  starting transfers between devices  2.55 us (1%)
    all_gather x1, waiting for transfers between devices, per_device(): lax.all_gather(key_rows, 'sp', axis=0, tiled=True)  42.9 us
    all_gather x1, waiting for transfers between devices, per_device(): lax.all_gather(values, 'sp', axis=0, tiled=True)  28.8 us
    all_gather x1, waiting for transfers between devices, per_device(): lax.all_gather(tokens, 'tp', axis=1, tiled=True)  25.2 us
    dot_general x4, matrix products, block_scores(): jnp.einsum('qhcd,khcd->hcqk', queries, key_block, preferred_element_type=...  20.8 us
    all_gather x1, waiting for transfers between devices, per_device(): lax.all_gather(conv_out, 'tp', axis=1, tiled=True)  16.8 us
    dot_general x6, matrix products, add_products(): jnp.dot(scaled, weight, preferred_element_type=jnp.float32)  10.6 us
    reduce_sum x2, other arithmetic, stats_step(): jnp.sum(exponent, axis=-1)  8.38 us
    all_gather x1, waiting for transfers between devices, per_device(): lax.all_gather(attn_out, 'tp', axis=1, tiled=True)  6.31 us
  transfers between devices with their start and end apart: 6, of which 6 were waited for; matrix products, arithmetic and copies ran while one was open for 15% of the time, Pallas kernels for 0%

commit v1 on v0

v1 whole, which is shorter than its diff:
```python
import functools

import jax
import jax.numpy as jnp
from jax import lax
from jax.experimental import pallas as pl
from jax.experimental.pallas import tpu as pltpu
from jax.sharding import PartitionSpec as P

NORM_EPS = 1e-06
HEAD_EPS = 1e-05
ROPE_BASE = 500000.0
MASKED = -1e30
HEAD_SCALE = 0.8
F32 = jnp.float32
BF16 = jnp.bfloat16


def dot(a, b):
    return jnp.dot(a, b, preferred_element_type=F32)


def dot_t(a, b):
    return lax.dot_general(a, b, (((1,), (1,)), ((), ())), preferred_element_type=F32)


def kernel(
    dims,
    tokens,
    gain,
    freq,
    wq_h,
    wk_h,
    wv_h,
    wo_h,
    wi_h,
    ws_h,
    taps,
    lambdas,
    head_gain,
    wa_h,
    wc_h,
    out,
    lse,
    tok,
    scaled,
    inv,
    cos_t,
    sin_t,
    wq,
    wk,
    wv,
    wo,
    wi,
    ws,
    wa,
    wc,
    kv,
    qz,
    row_max,
    row_sum,
    acc,
    gate,
    padded,
    tail,
    rim,
    conv_all,
    attn_all,
    total,
    w_sem,
    own_sem,
    tok_recv,
    tok_send,
    tok_relay,
    kv_recv,
    kv_send_z,
    kv_send_y,
    rim_sem,
    mix_recv,
    mix_send,
    mix_relay,
):
    S, T, Z, Y, H = dims["S"], dims["T"], dims["Z"], dims["Y"], dims["H"]
    L, Dt = tokens.shape
    Wd = T * Dt
    C = wq_h.shape[1]
    V = C // H
    hd = V // 2
    NR = tok_recv.shape[1]
    R = L // NR
    NM = mix_recv.shape[2]
    M = L // NM
    X = T // 2
    taps_n = taps.shape[0]
    PAD = tail.shape[0]

    sp = lax.axis_index("sp")
    tp = lax.axis_index("tp")
    z = sp // Y
    y = sp % Y
    core = tp % 2
    xi = tp // 2
    sib = xi * 2 + (1 - core)

    def peer(k):
        return ((xi + k) % X) * 2 + core

    def source(k):
        return ((xi - k + X) % X) * 2 + core

    pairs = [(wk_h, wk), (wv_h, wv), (wq_h, wq), (wi_h, wi), (ws_h, ws), (wo_h, wo), (wc_h, wc), (wa_h, wa)]
    own = pltpu.make_async_copy(tokens, tok.at[tp], own_sem)
    own.start()
    loads = [pltpu.make_async_copy(s, d, w_sem.at[i]) for i, (s, d) in enumerate(pairs)]
    for load in loads:
        load.start()

    barrier = pltpu.get_barrier_semaphore()

    def greet(target):
        pl.semaphore_signal(barrier, inc=1, device_id=target)

    for k in range(1, T):
        greet({"tp": (tp + k) % T})
    for k in range(1, Y):
        greet({"sp": z * Y + (y + k) % Y})
    has_up = z + 1 < Z
    has_down = z > 0
    far_up = jnp.logical_and(has_up, y == Y - 1) if Y > 1 else None
    far_down = jnp.logical_and(has_down, y == 0) if Y > 1 else None
    expect = (T - 1) + (Y - 1) + has_up.astype(jnp.int32) + has_down.astype(jnp.int32)

    @pl.when(has_up)
    def _():
        greet({"sp": sp + Y})

    @pl.when(has_down)
    def _():
        greet({"sp": sp - Y})

    if Y > 1:
        expect = expect + far_up.astype(jnp.int32) + far_down.astype(jnp.int32)

        @pl.when(far_up)
        def _():
            greet({"sp": sp + 1})

        @pl.when(far_down)
        def _():
            greet({"sp": sp - 1})

    pl.semaphore_wait(barrier, expect)

    def tok_rows(r):
        return pl.ds(pl.multiple_of(r * R, R), R)

    def tok_copy(src, piece, r, send, target):
        return pltpu.make_async_remote_copy(
            src_ref=src,
            dst_ref=tok.at[piece, tok_rows(r), :],
            send_sem=send,
            recv_sem=tok_recv.at[piece, r],
            device_id={"tp": target},
        )

    def tok_own(k, r):
        target = peer(k) if k else sib
        return tok_copy(tokens.at[tok_rows(r), :], tp, r, tok_send.at[k, r], target)

    def tok_forward(k, r):
        piece = source(k)
        return tok_copy(tok.at[piece, tok_rows(r), :], piece, r, tok_relay.at[k, r], sib)

    def tok_wait(piece, r):
        tok_copy(tok.at[piece, tok_rows(r), :], piece, r, tok_send.at[0, r], sib).wait_recv()

    for r in range(NR):
        for k in list(range(1, X)) + [0]:
            tok_own(k, r).start()

    lane = lax.broadcasted_iota(jnp.int32, (R, V), 1)
    first = (lane % hd) < (hd // 2)

    def table(r, carry):
        base = sp * L + r * R
        pos = (base + lax.broadcasted_iota(jnp.int32, (R, V), 0)).astype(F32)
        angle = pos * freq[...]
        sine = jnp.sin(angle)
        cos_t[tok_rows(r), :] = jnp.cos(angle)
        sin_t[tok_rows(r), :] = jnp.where(first, -sine, sine)
        return carry

    lax.fori_loop(0, NR, table, 0)

    def rotate(block, rows):
        low = (lax.broadcasted_iota(jnp.int32, block.shape, 1) % hd) < (hd // 2)
        other = jnp.where(
            low, pltpu.roll(block, V - hd // 2, 1), pltpu.roll(block, hd // 2, 1)
        )
        return block * cos_t[rows, :] + other * sin_t[rows, :]

    def kv_copy(j, r, send, target):
        block = kv.at[j, tok_rows(r), :]
        return pltpu.make_async_remote_copy(
            src_ref=block,
            dst_ref=block,
            send_sem=send,
            recv_sem=kv_recv.at[j, r],
            device_id={"sp": target},
        )

    def kv_up(dz, r):
        return kv_copy(sp - dz * Y, r, kv_send_z.at[dz, r], sp + Y)

    def kv_side(dz, r, k):
        return kv_copy(sp - dz * Y, r, kv_send_y.at[dz, r, k - 1], z * Y + (y + k) % Y)

    def kv_wait(j, r):
        kv_copy(j, r, kv_send_z.at[0, r], sp).wait_recv()

    def kv_send(dz, r, act):
        @pl.when(has_up)
        def _():
            act(kv_up(dz, r))

        for k in range(1, Y):

            @pl.when(jnp.logical_or(dz > 0, y + k < Y))
            def _():
                act(kv_side(dz, r, k))

    own.wait()
    loads[0].wait()
    loads[1].wait()

    def key_chunk(r, carry):
        rows = tok_rows(r)
        for k in range(1, X):
            tok_wait(source(k), r)
            tok_forward(k, r).start()
        tok_wait(sib, r)
        for k in range(1, X):
            tok_wait(((xi + k) % X) * 2 + (1 - core), r)
        squares = jnp.zeros((R, 1), F32)
        for t in range(T):
            block = tok[t, rows, :].astype(F32)
            squares = squares + jnp.sum(block * block, axis=1, keepdims=True)
            scaled[rows, t * Dt : (t + 1) * Dt] = (block * gain[t : t + 1, :]).astype(BF16)
        inverse = lax.rsqrt(squares / Wd + NORM_EPS)
        inv[rows, :] = inverse
        left = scaled[rows, :]
        keys = inverse * dot(left, wk[...])
        for h in range(H):
            kv[sp, rows, h * V : (h + 1) * V] = rotate(keys[:, h * V : (h + 1) * V], rows).astype(BF16)
        kv[sp, rows, C : 2 * C] = (inverse * dot(left, wv[...])).astype(BF16)
        kv_send(0, r, lambda copy: copy.start())
        return carry

    lax.fori_loop(0, NR, key_chunk, 0)

    for load in loads[2:6]:
        load.wait()
    half = lax.broadcasted_iota(jnp.int32, (M, V), 1) < hd
    scale = hd ** (-0.5)

    def mix_rows(r):
        return pl.ds(pl.multiple_of(r * M, M), M)

    def query_chunk(r, carry):
        rows = mix_rows(r)
        inverse = inv[rows, :]
        left = scaled[rows, :]
        queries = inverse * dot(left, wq[...])
        for h in range(H):
            turned = rotate(queries[:, h * V : (h + 1) * V], rows).astype(BF16).astype(F32) * scale
            qz[h, 0, rows, :] = jnp.where(half, turned, 0.0).astype(BF16)
            qz[h, 1, rows, :] = jnp.where(half, 0.0, turned).astype(BF16)
        inner = (inverse * dot(left, wi[...])).astype(BF16)
        signal = (inverse * dot(left, ws[...])).astype(BF16)
        conv_in = (inner.astype(F32) * signal.astype(F32)).astype(BF16)
        padded[pl.ds(pl.multiple_of(PAD + r * M, PAD), M), :] = conv_in.astype(F32)
        gate[rows, :] = (inverse * dot(left, wo[...])).astype(BF16)
        return carry

    lax.fori_loop(0, NM, query_chunk, 0)
    tail[...] = padded[L : L + PAD, :].astype(BF16)
    rim_copy = pltpu.make_async_remote_copy(
        src_ref=tail,
        dst_ref=rim,
        send_sem=rim_sem.at[0],
        recv_sem=rim_sem.at[1],
        device_id={"sp": (sp + 1) % S},
    )

    @pl.when(sp + 1 < S)
    def _():
        rim_copy.start()

    def attend(j, diagonal):
        def one(i, carry):
            rows = mix_rows(i)
            for h in range(H):
                query = qz[h, :, rows, :].reshape(2 * M, V)
                scores = dot_t(query, kv[j, :, h * V : (h + 1) * V])
                if diagonal:
                    row = lax.broadcasted_iota(jnp.int32, scores.shape, 0)
                    row = jnp.where(row >= M, row - M, row) + i * M
                    col = lax.broadcasted_iota(jnp.int32, scores.shape, 1)
                    scores = jnp.where(row >= col, scores, MASKED)
                    new_max = jnp.max(scores, axis=1, keepdims=True)
                else:
                    old_max = row_max[h, :, rows, :].reshape(2 * M, 1)
                    new_max = jnp.maximum(old_max, jnp.max(scores, axis=1, keepdims=True))
                weights = jnp.exp(scores - new_max)
                sums = jnp.sum(weights, axis=1, keepdims=True)
                mixed = dot(weights.astype(BF16), kv[j, :, C + h * V : C + (h + 1) * V])
                if not diagonal:
                    fade = jnp.exp(old_max - new_max)
                    sums = sums + fade * row_sum[h, :, rows, :].reshape(2 * M, 1)
                    mixed = mixed + fade * acc[h, :, rows, :].reshape(2 * M, V)
                row_max[h, :, rows, :] = new_max.reshape(2, M, 1)
                row_sum[h, :, rows, :] = sums.reshape(2, M, 1)
                acc[h, :, rows, :] = mixed.reshape(2, M, V)
            return carry

        lax.fori_loop(0, NM, one, 0)

    attend(sp, True)

    @pl.when(sp > 0)
    def _():
        rim_copy.wait_recv()
        padded[0:PAD, :] = rim[...].astype(F32)

    @pl.when(sp == 0)
    def _():
        padded[0:PAD, :] = jnp.zeros((PAD, C), F32)

    summed = jnp.zeros((L, C), F32)
    for j in range(taps_n):
        begin = PAD - (taps_n - 1) + j
        summed = summed + taps[j : j + 1, :] * padded[begin : begin + L, :]
    conv_all[tp, :, :] = (gate[...].astype(F32) * summed).astype(BF16)

    def mix_copy(which, buf, piece, r, send, target):
        block = buf.at[piece, mix_rows(r), :]
        return pltpu.make_async_remote_copy(
            src_ref=block,
            dst_ref=block,
            send_sem=send,
            recv_sem=mix_recv.at[which, piece, r],
            device_id={"tp": target},
        )

    def mix_own(which, buf, k, r):
        target = peer(k) if k else sib
        return mix_copy(which, buf, tp, r, mix_send.at[which, k, r], target)

    def mix_forward(which, buf, k, r):
        return mix_copy(which, buf, source(k), r, mix_relay.at[which, k, r], sib)

    def mix_wait(which, buf, piece, r):
        mix_copy(which, buf, piece, r, mix_send.at[which, 0, r], sib).wait_recv()

    for r in range(NM):
        for k in list(range(1, X)) + [0]:
            mix_own(0, conv_all, k, r).start()

    def step(dz, carry):
        @pl.when(dz <= z)
        def _():
            def forward(r, inner):
                kv_wait(sp - dz * Y, r)
                kv_send(dz, r, lambda copy: copy.start())
                return inner

            lax.fori_loop(0, NR, forward, 0)

        def row_block(k, inner):
            side = (y + k) % Y
            level = jnp.where(k == 0, z - dz, z - dz + 1)
            j = level * Y + side
            valid = jnp.where(k == 0, dz <= z, jnp.logical_or(level < z, side < y))

            @pl.when(valid)
            def _():
                @pl.when(k > 0)
                def _():
                    for r in range(NR):
                        kv_wait(j, r)

                attend(j, False)

            return inner

        lax.fori_loop(0, Y, row_block, 0)
        return carry

    lax.fori_loop(1, z + 2, step, 0)

    def finish(i, carry):
        rows = mix_rows(i)
        for h in range(H):
            first_map = acc[h, 0, rows, :] / row_sum[h, 0, rows, :]
            second_map = acc[h, 1, rows, :] / row_sum[h, 1, rows, :]
            head_mix = first_map - lambdas[h] * second_map
            mean = jnp.mean(head_mix * head_mix, axis=1, keepdims=True)
            normed = head_mix * lax.rsqrt(mean + HEAD_EPS) * head_gain[...] * HEAD_SCALE
            attn_all[tp, rows, h * V : (h + 1) * V] = normed.astype(BF16)
        for k in list(range(1, X)) + [0]:
            mix_own(1, attn_all, k, i).start()
        return carry

    lax.fori_loop(0, NM, finish, 0)

    loads[6].wait()
    loads[7].wait()

    def gather(which, buf, r):
        for k in range(1, X):
            mix_wait(which, buf, source(k), r)
            mix_forward(which, buf, k, r).start()

    def gather_rest(which, buf, r):
        mix_wait(which, buf, sib, r)
        for k in range(1, X):
            mix_wait(which, buf, ((xi + k) % X) * 2 + (1 - core), r)

    def conv_part(r, carry):
        rows = mix_rows(r)
        gather(0, conv_all, r)
        gather_rest(0, conv_all, r)
        part = dot(conv_all[0, rows, :], wc[0:C, :])
        for t in range(1, T):
            part = part + dot(conv_all[t, rows, :], wc[t * C : (t + 1) * C, :])
        total[rows, :] = part
        return carry

    lax.fori_loop(0, NM, conv_part, 0)

    lanes = lax.broadcasted_iota(jnp.int32, (L, 128), 1)
    columns = jnp.zeros((L, 128), F32)
    for h in range(H):
        for c in range(2):
            value = row_max[h, c, :, :] + jnp.log(row_sum[h, c, :, :])
            columns = jnp.where(lanes == 2 * h + c, value, columns)
    lse[...] = jnp.transpose(columns)[0 : 2 * H, :]

    def attn_part(r, carry):
        rows = mix_rows(r)
        gather(1, attn_all, r)
        gather_rest(1, attn_all, r)
        part = total[rows, :]
        for t in range(T):
            part = part + dot(attn_all[t, rows, :], wa[t * C : (t + 1) * C, :])
        out[rows, :] = part.astype(BF16)
        return carry

    lax.fori_loop(0, NM, attn_part, 0)

    for r in range(NR):
        for k in range(X):
            tok_own(k, r).wait_send()
        for k in range(1, X):
            tok_forward(k, r).wait_send()

    def drain(dz, carry):
        def inner(r, c):
            kv_send(dz, r, lambda copy: copy.wait_send())
            return c

        return lax.fori_loop(0, NR, inner, carry)

    lax.fori_loop(0, z + 1, drain, 0)
    for which, buf in ((0, conv_all), (1, attn_all)):
        for r in range(NM):
            for k in range(X):
                mix_own(which, buf, k, r).wait_send()
            for k in range(1, X):
                mix_forward(which, buf, k, r).wait_send()

    @pl.when(sp + 1 < S)
    def _():
        rim_copy.wait_send()


def per_device(
    dims,
    tokens,
    norm_gain,
    query_weight,
    key_weight,
    value_weight,
    outer_gate_weight,
    inner_gate_weight,
    conv_input_weight,
    conv_taps,
    lambdas,
    head_gain,
    attn_out_weight,
    conv_out_weight,
):
    S, T, Z, Y = dims["S"], dims["T"], dims["Z"], dims["Y"]
    L, Dt = tokens.shape
    H = lambdas.shape[0]
    C = query_weight.shape[1]
    V = C // H
    hd = V // 2
    O = attn_out_weight.shape[1]
    Wd = norm_gain.shape[0]
    NR, NM, PAD = 4, 2, 16
    X = T // 2
    frequency = ROPE_BASE ** (-jnp.arange(hd // 2, dtype=F32) * 2.0 / hd)
    freq = jnp.tile(frequency, 4)[None, :]
    any_spec = pl.BlockSpec(memory_space=pl.ANY)
    vmem = pl.BlockSpec(memory_space=pltpu.VMEM)
    smem = pl.BlockSpec(memory_space=pltpu.SMEM)
    dma = pltpu.SemaphoreType.DMA
    mixed, lse = pl.pallas_call(
        functools.partial(kernel, dict(dims, H=H)),
        out_shape=(
            jax.ShapeDtypeStruct((L, O), BF16),
            jax.ShapeDtypeStruct((2 * H, L), F32),
        ),
        in_specs=[any_spec, vmem, vmem] + [any_spec] * 6 + [vmem, smem, vmem] + [any_spec] * 2,
        out_specs=(vmem, vmem),
        scratch_shapes=[
            pltpu.VMEM((T, L, Dt), BF16),
            pltpu.VMEM((L, Wd), BF16),
            pltpu.VMEM((L, 1), F32),
            pltpu.VMEM((L, V), F32),
            pltpu.VMEM((L, V), F32),
        ]
        + [pltpu.VMEM((Wd, C), BF16)] * 6
        + [pltpu.VMEM((T * C, O), BF16)] * 2
        + [
            pltpu.VMEM((S, L, 2 * C), BF16),
            pltpu.VMEM((H, 2, L, V), BF16),
            pltpu.VMEM((H, 2, L, 1), F32),
            pltpu.VMEM((H, 2, L, 1), F32),
            pltpu.VMEM((H, 2, L, V), F32),
            pltpu.VMEM((L, C), BF16),
            pltpu.VMEM((PAD + L, C), F32),
            pltpu.VMEM((PAD, C), BF16),
            pltpu.VMEM((PAD, C), BF16),
            pltpu.VMEM((T, L, C), BF16),
            pltpu.VMEM((T, L, C), BF16),
            pltpu.VMEM((L, O), F32),
            dma((8,)),
            dma,
            dma((T, NR)),
            dma((X, NR)),
            dma((X, NR)),
            dma((S, NR)),
            dma((Z, NR)),
            dma((Z, NR, max(Y - 1, 1))),
            dma((2,)),
            dma((2, T, NM)),
            dma((2, X, NM)),
            dma((2, X, NM)),
        ],
        compiler_params=pltpu.CompilerParams(
            collective_id=0, has_side_effects=True, vmem_limit_bytes=60 * 1024 * 1024
        ),
        name="mixer",
    )(
        tokens,
        norm_gain.reshape(T, Dt),
        freq,
        query_weight,
        key_weight,
        value_weight,
        outer_gate_weight,
        inner_gate_weight,
        conv_input_weight,
        conv_taps,
        lambdas,
        head_gain[None, :],
        attn_out_weight,
        conv_out_weight,
    )
    return mixed, lse.reshape(H, 2, L)


def solution(mesh):
    S, T = mesh.shape["sp"], mesh.shape["tp"]
    Y = max(d for d in range(1, S + 1) if S % d == 0 and d * d <= S)
    dims = {"S": S, "T": T, "Z": S // Y, "Y": Y}
    in_specs = (
        P("sp", "tp"),
        P(),
        P(None, "tp"),
        P(None, "tp"),
        P(None, "tp"),
        P(None, "tp"),
        P(None, "tp"),
        P(None, "tp"),
        P(None, "tp"),
        P("tp"),
        P(),
        P(None, "tp"),
        P(None, "tp"),
    )
    out_specs = (P("sp", "tp"), P("tp", None, "sp"))
    return jax.shard_map(
        functools.partial(per_device, dims),
        mesh=mesh,
        in_specs=in_specs,
        out_specs=out_specs,
        check_vma=False,
    )
```

time: 212 us -> 80.3 us (0.38)
  waiting for transfers between devices: 124 us -> 0 us
  Pallas kernels: 0 us -> 74.9 us
  matrix products: 38.8 us -> 0 us
  other arithmetic: 19.3 us -> 0.01 us
  between operations: 14.1 us -> 0.66 us
  local copies, waits for them, and re-layouts: 7.83 us -> 4.45 us
  loops' own time: 2.83 us -> 0 us
  starting transfers between devices: 2.55 us -> 0 us
    all_gather x5 -> x0, waiting for transfers between devices: 120 us -> none  [the longest x1 42.9 us: per_device(): lax.all_gather(key_rows, 'sp', axis=0, tiled=True)]
    pallas_call x0 -> x1, Pallas kernels: none -> 74.9 us  [per_device(): pl.pallas_call(functools.partial(kernel, dict(dims, H=H)), out_shape=(jax...]
    dot_general x14 -> x0, matrix products: 38.8 us -> none  [the longest x4 20.8 us: block_scores(): jnp.einsum('qhcd,khcd->hcqk', queries, key_block, preferred_element_type=...]
    reduce_sum x4 -> x0, other arithmetic: 11.7 us -> none  [the longest x2 8.38 us: stats_step(): jnp.sum(exponent, axis=-1)]
    ppermute x1 -> x0, waiting for transfers between devices: 3.71 us -> none  [shifted(): return lax.ppermute(block, axis, route)]
    ge x4 -> x0, other arithmetic: 3.05 us -> none  [block_scores(): query_pos[:, None]]
    another operation x2 -> x0, loops' own time: 2.83 us -> none  [over_shards(): lax.scan(scan_step, running, (stacked, jnp.arange(steps_count, dtype=jnp....]
    dynamic_slice x4 -> x0, local copies, waits for them, and re-layouts: 2.52 us -> none  [over_shards(): lax.scan(scan_step, running, (stacked, jnp.arange(steps_count, dtype=jnp....]
  transfers between devices with their start and end apart: 6 -> 0, of which waited for: 6 -> 0; matrix products, arithmetic and copies ran while one was open for 15% -> 0% of each run, Pallas kernels for 0% -> 0%
where the time goes in v1:
time: 80.3 us; the launch traced here: 80 us
  Pallas kernels  74.9 us (93%)
  local copies, waits for them, and re-layouts  4.45 us (6%)
    pallas_call x1, Pallas kernels, per_device(): pl.pallas_call(functools.partial(kernel, dict(dims, H=H)), out_shape=(jax...  74.9 us
    unnamed x3, local copies, waits for them, and re-layouts  1.94 us

profile of v1, /device:TPU:25, one launch (start us, length us, event | category | flops | bytes accessed | tf_op | source)
XLA Modules:
  0.0 80.0 jit_solution(10665235472780423575)
XLA Ops:
  0.6 0.0 copy-start
  0.7 0.6 broadcast_in_dim_tile.3.freq
  1.3 0.1 copy-done
  1.3 0.6 reshape.16.gain
  1.9 74.9 %mixer.1 = (bf16[512,512]{1,0:T(8,128)(2,1)}, f32[4,512]{1,0:T(4,128)}) custom-call(bf16[512,512]{1,0:T(8,128)(2,1)} %tokens.1, f32[4,512]{1,0:T(4,128)} %reshape.16.gain, f32[1,128]{1,0:T(1,128)} %broadcast_in_dim_tile.3.freq, bf16[2048,256]{1,0:T(8,128)(2,1)} %wq_h.1, bf16[2048,256]{1,0:T(8,128)(2,1)} %wk_h.1, bf16[2048,256]{1,0:T(8,128)(2,1)} %wv_h.1, ...), custom_call_target="tpu_custom_call" | custom-call | tf_op jit(solution)/shard_map/mixer/pallas_call | solution.py:519
  76.9 1.3 %reshape.17 = f32[2,2,512]{2,1,0:T(2,128)} reshape(f32[4,512]{1,0:T(4,128)} %get-tuple-element.5) | data formatting | bytes 16384 | tf_op jit(solution)/shard_map/reshape | solution.py:582
  78.2 1.9 %copy.16 = bf16[512,512]{1,0:T(8,128)(2,1)} copy(bf16[512,512]{1,0:T(8,128)(2,1)} %get-tuple-element.8) | data formatting | bytes 1048576
  (2 shorter events, 0.0 us)
Async XLA Ops:
  0.6 0.7 copy-start

commit v2 on v1

--- a/solution.py
+++ b/solution.py
@@ -2,6 +2,7 @@
 
 import jax
 import jax.numpy as jnp
+import numpy as np
 from jax import lax
 from jax.experimental import pallas as pl
 from jax.experimental.pallas import tpu as pltpu
@@ -75,6 +76,7 @@
     kv_recv,
     kv_send_z,
     kv_send_y,
+    kv_extra,
     rim_sem,
     mix_recv,
     mix_send,
@@ -218,16 +220,43 @@
     def kv_wait(j, r):
         kv_copy(j, r, kv_send_z.at[0, r], sp).wait_recv()
 
+    EX = NR // 2 if Y == 2 else 0
+
+    def extra(r):
+        return kv_copy(0, r, kv_extra.at[r], sp + Y)
+
     def kv_send(dz, r, act):
         @pl.when(has_up)
         def _():
             act(kv_up(dz, r))
 
         for k in range(1, Y):
-
-            @pl.when(jnp.logical_or(dz > 0, y + k < Y))
+            wanted = jnp.logical_or(dz > 0, y + k < Y)
+            if EX:
+                other_way = jnp.logical_and(dz == z, jnp.logical_and(dz > 0, r < EX))
+                wanted = jnp.logical_and(wanted, jnp.logical_not(jnp.logical_and(y == 0, other_way)))
+
+            @pl.when(wanted)
             def _():
                 act(kv_side(dz, r, k))
+
+    def relay(dz, r):
+        @pl.when(dz <= z)
+        def _():
+            kv_wait(sp - dz * Y, r)
+            kv_send(dz, r, lambda copy: copy.start())
+
+    def first_relay(r):
+        relay(1, r)
+        if EX:
+
+            @pl.when(jnp.logical_and(jnp.logical_and(z == 0, y == 1), r < EX))
+            def _():
+                kv_wait(0, r)
+
+                @pl.when(has_up)
+                def _():
+                    extra(r).start()
 
     own.wait()
     loads[0].wait()
@@ -245,7 +274,7 @@
         for t in range(T):
             block = tok[t, rows, :].astype(F32)
             squares = squares + jnp.sum(block * block, axis=1, keepdims=True)
-            scaled[rows, t * Dt : (t + 1) * Dt] = (block * gain[t : t + 1, :]).astype(BF16)
+            scaled[rows, t * Dt : (t + 1) * Dt] = (block * gain[:, t * Dt : (t + 1) * Dt]).astype(BF16)
         inverse = lax.rsqrt(squares / Wd + NORM_EPS)
         inv[rows, :] = inverse
         left = scaled[rows, :]
@@ -254,6 +283,11 @@
             kv[sp, rows, h * V : (h + 1) * V] = rotate(keys[:, h * V : (h + 1) * V], rows).astype(BF16)
         kv[sp, rows, C : 2 * C] = (inverse * dot(left, wv[...])).astype(BF16)
         kv_send(0, r, lambda copy: copy.start())
+
+        @pl.when(r > 0)
+        def _():
+            first_relay(r - 1)
+
         return carry
 
     lax.fori_loop(0, NR, key_chunk, 0)
@@ -280,6 +314,11 @@
         conv_in = (inner.astype(F32) * signal.astype(F32)).astype(BF16)
         padded[pl.ds(pl.multiple_of(PAD + r * M, PAD), M), :] = conv_in.astype(F32)
         gate[rows, :] = (inverse * dot(left, wo[...])).astype(BF16)
+
+        @pl.when(r == 0)
+        def _():
+            first_relay(NR - 1)
+
         return carry
 
     lax.fori_loop(0, NM, query_chunk, 0)
@@ -367,16 +406,12 @@
             mix_own(0, conv_all, k, r).start()
 
     def step(dz, carry):
-        @pl.when(dz <= z)
-        def _():
-            def forward(r, inner):
-                kv_wait(sp - dz * Y, r)
-                kv_send(dz, r, lambda copy: copy.start())
-                return inner
-
-            lax.fori_loop(0, NR, forward, 0)
-
         def row_block(k, inner):
+            def forward(r, c):
+                relay(dz + 1, r)
+                return c
+
+            lax.fori_loop(k * NR // Y, (k + 1) * NR // Y, forward, 0)
             side = (y + k) % Y
             level = jnp.where(k == 0, z - dz, z - dz + 1)
             j = level * Y + side
@@ -387,7 +422,19 @@
                 @pl.when(k > 0)
                 def _():
                     for r in range(NR):
-                        kv_wait(j, r)
+                        if r < EX:
+                            climbs = jnp.logical_and(level == 0, y == 1)
+
+                            @pl.when(jnp.logical_not(jnp.logical_and(climbs, z == 0)))
+                            def _():
+                                kv_wait(j, r)
+
+                            @pl.when(jnp.logical_and(climbs, jnp.logical_and(z > 0, has_up)))
+                            def _():
+                                extra(r).start()
+
+                        else:
+                            kv_wait(j, r)
 
                 attend(j, False)
 
@@ -444,7 +491,9 @@
         for c in range(2):
             value = row_max[h, c, :, :] + jnp.log(row_sum[h, c, :, :])
             columns = jnp.where(lanes == 2 * h + c, value, columns)
-    lse[...] = jnp.transpose(columns)[0 : 2 * H, :]
+    turned_columns = jnp.transpose(columns)
+    for h in range(H):
+        lse[h] = turned_columns[2 * h : 2 * h + 2, :]
 
     def attn_part(r, carry):
         rows = mix_rows(r)
@@ -472,6 +521,13 @@
         return lax.fori_loop(0, NR, inner, carry)
 
     lax.fori_loop(0, z + 1, drain, 0)
+    if EX:
+
+        @pl.when(jnp.logical_and(y == 1, has_up))
+        def _():
+            for r in range(EX):
+                extra(r).wait_send()
+
     for which, buf in ((0, conv_all), (1, attn_all)):
         for r in range(NM):
             for k in range(X):
@@ -510,8 +566,8 @@
     Wd = norm_gain.shape[0]
     NR, NM, PAD = 4, 2, 16
     X = T // 2
-    frequency = ROPE_BASE ** (-jnp.arange(hd // 2, dtype=F32) * 2.0 / hd)
-    freq = jnp.tile(frequency, 4)[None, :]
+    frequency = ROPE_BASE ** (-np.arange(hd // 2) * 2.0 / hd)
+    freq = jnp.asarray(np.tile(frequency, 4)[None, :], F32)
     any_spec = pl.BlockSpec(memory_space=pl.ANY)
     vmem = pl.BlockSpec(memory_space=pltpu.VMEM)
     smem = pl.BlockSpec(memory_space=pltpu.SMEM)
@@ -520,7 +576,7 @@
         functools.partial(kernel, dict(dims, H=H)),
         out_shape=(
             jax.ShapeDtypeStruct((L, O), BF16),
-            jax.ShapeDtypeStruct((2 * H, L), F32),
+            jax.ShapeDtypeStruct((H, 2, L), F32),
         ),
         in_specs=[any_spec, vmem, vmem] + [any_spec] * 6 + [vmem, smem, vmem] + [any_spec] * 2,
         out_specs=(vmem, vmem),
@@ -554,6 +610,7 @@
             dma((S, NR)),
             dma((Z, NR)),
             dma((Z, NR, max(Y - 1, 1))),
+            dma((NR,)),
             dma((2,)),
             dma((2, T, NM)),
             dma((2, X, NM)),
@@ -565,7 +622,7 @@
         name="mixer",
     )(
         tokens,
-        norm_gain.reshape(T, Dt),
+        norm_gain[None, :],
         freq,
         query_weight,
         key_weight,
@@ -579,7 +636,7 @@
         attn_out_weight,
         conv_out_weight,
     )
-    return mixed, lse.reshape(H, 2, L)
+    return mixed, lse
 
 
 def solution(mesh):

time: 80.3 us -> 78.3 us (0.975)
  local copies, waits for them, and re-layouts: 4.45 us -> 2.48 us
    reshape x2 -> x0, local copies, waits for them, and re-layouts: 1.92 us -> none  [the longest x1 1.31 us: per_device(): return (mixed, lse.reshape(H, 2, L))]
    unnamed x3 -> x4, local copies, waits for them, and re-layouts: 1.94 us -> 2.48 us
where the time goes in v2:
time: 78.3 us; the launch traced here: 78.1 us
  Pallas kernels  75 us (96%)
  local copies, waits for them, and re-layouts  2.48 us (3%)
    pallas_call x1, Pallas kernels, per_device(): pl.pallas_call(functools.partial(kernel, dict(dims, H=H)), out_shape=(jax...  75 us
    unnamed x4, local copies, waits for them, and re-layouts  2.48 us

profile of v2, /device:TPU:25, one launch (start us, length us, event | category | flops | bytes accessed | tf_op | source)
XLA Modules:
  0.0 78.1 jit_solution(17531902746700963711)
XLA Ops:
  0.6 75.0 %mixer.1 = (bf16[512,512]{1,0:T(8,128)(2,1)}, f32[2,2,512]{2,1,0:T(2,128)}) custom-call(bf16[512,512]{1,0:T(8,128)(2,1)} %tokens.1, f32[1,2048]{1,0:T(1,128)} %bitcast.2, f32[1,128]{1,0:T(1,128)} %constant.2.clone.freq, bf16[2048,256]{1,0:T(8,128)(2,1)} %wq_h.1, bf16[2048,256]{1,0:T(8,128)(2,1)} %wk_h.1, bf16[2048,256]{1,0:T(8,128)(2,1)} %wv_h.1, ...), custom_call_target="tpu_custom_call" | custom-call | tf_op jit(solution)/shard_map/mixer/pallas_call | solution.py:575
  75.7 0.0 copy-start
  75.7 1.9 %copy.18 = bf16[512,512]{1,0:T(8,128)(2,1)} copy(bf16[512,512]{1,0:T(8,128)(2,1)} %get-tuple-element.4) | data formatting | bytes 1048576
  77.5 0.0 copy-done
  77.5 0.6 copy.19
Async XLA Ops:
  75.7 1.9 %copy-start = (f32[2,2,512]{2,1,0:T(2,128)S(1)}, f32[2,2,512]{2,1,0:T(2,128)}, u32[]{:S(2)}) copy-start(f32[2,2,512]{2,1,0:T(2,128)} %get-tuple-element.5) | copy-start | bytes 24580
